TPU v7x, 32 devices: a whole 2x2x4 slice. The times are simulated.
32 devices in a mesh: grp: 2 (over x), sp: 4 (over y, core), tp: 4 (over z).
Axes of the slice: x: 2, y: 2, z: 4, core: 2. Of those that a mesh axis runs over, the one named last changes fastest.
Arguments:
- tokens_in: bfloat16 [2048, 2048], P(('grp', 'sp'), 'tp'), parts along dimension 0, may hold values from -8 to 8
- out_gate: bfloat16 [3, 2048, 2048], P(None, 'sp', 'tp'), may hold values from -0.125 to 0.125
- in_gate: bfloat16 [3, 2048, 2048], P(None, 'sp', 'tp'), may hold values from -0.125 to 0.125
- value_proj: bfloat16 [3, 2048, 2048], P(None, 'sp', 'tp'), may hold values from -0.125 to 0.125
- mix_proj: bfloat16 [3, 2048, 2048], P(None, 'sp', 'tp'), may hold values from -0.125 to 0.125
- conv_taps: float32 [3, 3, 2048], P(None, None, 'tp'), may hold values from -3.5 to 3.5
- norm_gains: float32 [3, 2048], P(None, 'tp'), may hold values from 0.1 to 1.9
- final_gain: float32 [2048], P('tp'), may hold values from 0.1 to 1.9
Outputs:
- normed_out: bfloat16 [2048, 2048], P(('grp', 'sp'), 'tp'), parts along dimension 0
There are 2 independent parts, one for each index of `grp`. A program takes and returns all parts, laid end to end along the dimension named above; an argument that names none is the same for every part. Nothing has to cross between parts.
All inputs are finite; a program needn't handle non-finite values.
Results may differ from a plain program's by a relative error of at most 0.025.
Values may be sent and summed in bfloat16 or wider, within the bound.
A program may use at most 64 MiB of HBM per device.

v0:
```python
import jax
import jax.numpy as jnp
from jax import lax
from jax.sharding import PartitionSpec as P

D = 2048
TAPS = 3
LAYERS = 3
epsilon = 1e-06


def passed_along(shard, axis, by):
    peers = lax.axis_size(axis)
    pairs = [(i, i + by) for i in range(peers) if 0 <= i + by < peers]
    return lax.ppermute(shard, axis, pairs)


def row_scale(stream):
    squares = lax.psum(jnp.sum(stream * stream, axis=1, keepdims=True), "tp")
    return lax.rsqrt(squares / D + epsilon)


def shards(tokens_in, out_gate, in_gate, value_proj, mix_proj, conv_taps, norm_gains, final_gain):
    stream = tokens_in.astype(jnp.float32)
    row_count = stream.shape[0]
    reach = TAPS - 1
    whole = (
        lax.all_gather(out_gate, "sp", axis=1, tiled=True),
        lax.all_gather(in_gate, "sp", axis=1, tiled=True),
        lax.all_gather(value_proj, "sp", axis=1, tiled=True),
        lax.all_gather(mix_proj, "sp", axis=1, tiled=True),
    )
    for layer_index in range(LAYERS):
        scale = row_scale(stream)
        normed = (stream * norm_gains[layer_index]).astype(jnp.bfloat16)
        gathered = lax.all_gather(normed, "tp", axis=1, tiled=True)
        products = tuple(
            (
                jnp.dot(gathered, weight[layer_index], preferred_element_type=jnp.float32)
                for weight in whole[:3]
            )
        )
        out_gates, in_gates, values = [
            (product * scale).astype(jnp.bfloat16) for product in products
        ]
        product_v = (in_gates.astype(jnp.float32) * values.astype(jnp.float32)).astype(jnp.bfloat16)
        earlier = passed_along(product_v[row_count - reach :], "sp", 1)
        padded = jnp.concatenate([earlier, product_v], axis=0)
        convolved = padded[0:row_count].astype(jnp.float32) * conv_taps[layer_index, 0]
        for tap_index in range(1, TAPS):
            convolved = (
                convolved
                + padded[tap_index : tap_index + row_count].astype(jnp.float32)
                * conv_taps[layer_index, tap_index]
            )
        gated = (out_gates.astype(jnp.float32) * convolved).astype(jnp.bfloat16)
        spread = lax.all_gather(gated, "tp", axis=1, tiled=True)
        mixed = jnp.dot(spread, whole[3][layer_index], preferred_element_type=jnp.float32)
        stream = stream + mixed
    scale = row_scale(stream)
    return (stream * scale * final_gain).astype(jnp.bfloat16)


def solution(mesh):
    in_specs = (
        P(("grp", "sp"), "tp"),
        P(None, "sp", "tp"),
        P(None, "sp", "tp"),
        P(None, "sp", "tp"),
        P(None, "sp", "tp"),
        P(None, None, "tp"),
        P(None, "tp"),
        P("tp"),
    )
    out_specs = P(("grp", "sp"), "tp")
    return jax.shard_map(shards, mesh=mesh, in_specs=in_specs, out_specs=out_specs, check_vma=False)
```

profile of v0, /device:TPU:0, one launch (start us, length us, event | category | flops | bytes accessed | tf_op | source)
XLA Modules:
  0.0 424.5 jit_solution(9574232206159354128)
XLA Ops:
  6.5 0.0 all-gather.11.cloned.1.call-start
  6.5 0.8 fusion.60
  7.4 1.7 fusion.55
  9.1 0.0 all-gather.11.cloned.1.call-update
  9.1 0.0 all-gather.17.cloned.1.call-start
  9.2 0.7 all-gather.17.cloned.1.call-update
  9.9 0.0 all-gather.15.cloned.1.call-start
  9.9 0.7 all-gather.15.cloned.1.call-update
  10.6 0.0 copy-start.1
  10.6 0.0 all-gather.13.cloned.1.call-start
  10.7 0.5 all-gather.13.cloned.1.call-update
  11.2 0.0 all-gather.21.cloned.1.call-start
  11.2 0.5 all-gather.21.cloned.1.call-update
  11.8 0.0 all-gather.19.cloned.1.call-start
  11.8 13.5 %psum.28 = f32[256,1]{0,1:T(1,128)S(1)} all-reduce(f32[256,1]{0,1:T(1,128)S(1)} %bitcast.159), channel_id=1, replica_groups=mesh['grp'=2,'sp'=4,'tp'=4] {'tp'}, use_global_device_ids=true, to_apply=%region_1.0 | all-reduce | flops 256 | bytes 2048 | tf_op jit(solution)/shard_map/psum | solution.py:19
  25.3 14.7 %all-gather.11.cloned.1.call-done = bf16[256,2048]{1,0:T(8,128)(2,1)} async-done(((bf16[256,512]{1,0:T(8,128)(2,1)}), bf16[256,2048]{1,0:T(8,128)(2,1)}) %all-gather.11.cloned.1.call-update) | async-done | bytes 1048592 | tf_op jit(solution)/shard_map/all_gather | solution.py:36
  40.0 47.3 %all-gather.17.cloned.1.call-done = bf16[3,2048,512]{2,1,0:T(8,128)(2,1)} async-done(((bf16[3,512,512]{2,1,0:T(8,128)(2,1)}), bf16[3,2048,512]{2,1,0:T(8,128)(2,1)}) %all-gather.17.cloned.1.call-update) | async-done | bytes 6291472 | tf_op jit(solution)/shard_map/all_gather | solution.py:30
  87.3 2.6 fusion.39
  90.0 0.0 copy-start
  90.0 45.3 %all-gather.15.cloned.1.call-done = bf16[3,2048,512]{2,1,0:T(8,128)(2,1)} async-done(((bf16[3,512,512]{2,1,0:T(8,128)(2,1)}), bf16[3,2048,512]{2,1,0:T(8,128)(2,1)}) %all-gather.15.cloned.1.call-update) | async-done | bytes 6291472 | tf_op jit(solution)/shard_map/all_gather | solution.py:29
  135.3 2.6 fusion.38
  137.9 2.2 collective-permute-start
  140.1 0.0 copy-done.1
  140.1 43.0 %all-gather.13.cloned.1.call-done = bf16[3,2048,512]{2,1,0:T(8,128)(2,1)} async-done(((bf16[3,512,512]{2,1,0:T(8,128)(2,1)}), bf16[3,2048,512]{2,1,0:T(8,128)(2,1)}) %all-gather.13.cloned.1.call-update) | async-done | bytes 6291472 | tf_op jit(solution)/shard_map/all_gather | solution.py:28
  183.1 0.0 collective-permute-done
  183.1 0.0 copy-done.3
  183.1 3.1 fusion.35
  186.2 0.0 all-gather.19.cloned.1.call-update
  186.2 0.0 all-gather.23.cloned.1.call-start
  186.3 44.6 %all-gather.21.cloned.1.call-done = bf16[3,2048,512]{2,1,0:T(8,128)(2,1)} async-done(((bf16[3,512,512]{2,1,0:T(8,128)(2,1)}), bf16[3,2048,512]{2,1,0:T(8,128)(2,1)}) %all-gather.21.cloned.1.call-update) | async-done | bytes 6291472 | tf_op jit(solution)/shard_map/all_gather | solution.py:31
  230.9 29.4 %all-gather.19.cloned.1.call-done = bf16[256,2048]{1,0:T(8,128)(2,1)} async-done(((bf16[256,512]{1,0:T(8,128)(2,1)}), bf16[256,2048]{1,0:T(8,128)(2,1)}) %all-gather.19.cloned.1.call-update) | async-done | bytes 1048592 | tf_op jit(solution)/shard_map/all_gather | solution.py:57
  260.3 0.0 copy-done
  260.3 3.4 multiply_reduce_fusion.2
  263.7 0.0 all-gather.23.cloned.1.call-update
  263.7 0.0 all-gather.25.cloned.1.call-start
  263.8 10.3 %psum.29 = f32[256,1]{0,1:T(1,128)S(1)} all-reduce(f32[256,1]{0,1:T(1,128)S(1)} %bitcast.182), channel_id=1, replica_groups=mesh['grp'=2,'sp'=4,'tp'=4] {'tp'}, use_global_device_ids=true, to_apply=%region_3.0 | all-reduce | flops 256 | bytes 2048 | tf_op jit(solution)/shard_map/psum | solution.py:19
  274.1 17.2 %all-gather.23.cloned.1.call-done = bf16[256,2048]{1,0:T(8,128)(2,1)} async-done(((bf16[256,512]{1,0:T(8,128)(2,1)}), bf16[256,2048]{1,0:T(8,128)(2,1)}) %all-gather.23.cloned.1.call-update) | async-done | bytes 1048592 | tf_op jit(solution)/shard_map/all_gather | solution.py:36
  291.2 2.7 fusion.46
  293.9 2.6 fusion.45
  296.6 1.3 collective-permute-start.1
  297.9 0.8 collective-permute-done.1
  298.7 0.0 copy-done.5
  298.7 3.1 fusion.42
  301.8 0.0 all-gather.25.cloned.1.call-update
  301.8 0.0 all-gather.27.cloned.1.call-start
  301.9 30.3 %all-gather.25.cloned.1.call-done = bf16[256,2048]{1,0:T(8,128)(2,1)} async-done(((bf16[256,512]{1,0:T(8,128)(2,1)}), bf16[256,2048]{1,0:T(8,128)(2,1)}) %all-gather.25.cloned.1.call-update) | async-done | bytes 1048592 | tf_op jit(solution)/shard_map/all_gather | solution.py:57
  332.2 3.3 multiply_reduce_fusion.1
  335.5 0.0 all-gather.27.cloned.1.call-update
  335.5 0.0 all-gather.29.cloned.1.call-start
  335.6 10.3 %psum.30 = f32[256,1]{0,1:T(1,128)S(1)} all-reduce(f32[256,1]{0,1:T(1,128)S(1)} %bitcast.181), channel_id=1, replica_groups=mesh['grp'=2,'sp'=4,'tp'=4] {'tp'}, use_global_device_ids=true, to_apply=%region_5.0 | all-reduce | flops 256 | bytes 2048 | tf_op jit(solution)/shard_map/psum | solution.py:19
  345.9 17.2 %all-gather.27.cloned.1.call-done = bf16[256,2048]{1,0:T(8,128)(2,1)} async-done(((bf16[256,512]{1,0:T(8,128)(2,1)}), bf16[256,2048]{1,0:T(8,128)(2,1)}) %all-gather.27.cloned.1.call-update) | async-done | bytes 1048592 | tf_op jit(solution)/shard_map/all_gather | solution.py:36
  363.0 2.7 fusion.53
  365.7 2.6 fusion.52
  368.4 0.0 copy-start.2
  368.4 1.3 collective-permute-start.2
  369.7 0.8 collective-permute-done.2
  370.5 0.0 copy-done.4
  370.5 3.1 fusion.49
  373.6 0.0 all-gather.29.cloned.1.call-update
  373.6 30.3 %all-gather.29.cloned.1.call-done = bf16[256,2048]{1,0:T(8,128)(2,1)} async-done(((bf16[256,512]{1,0:T(8,128)(2,1)}), bf16[256,2048]{1,0:T(8,128)(2,1)}) %all-gather.29.cloned.1.call-update) | async-done | bytes 1048592 | tf_op jit(solution)/shard_map/all_gather | solution.py:57
  404.0 2.7 multiply_reduce_fusion
  406.7 10.2 %psum.31 = f32[256,1]{0,1:T(1,128)S(1)} all-reduce(f32[256,1]{0,1:T(1,128)S(1)} %bitcast.183), channel_id=1, replica_groups=mesh['grp'=2,'sp'=4,'tp'=4] {'tp'}, use_global_device_ids=true, to_apply=%region_7.0 | all-reduce | flops 256 | bytes 2048 | tf_op jit(solution)/shard_map/psum | solution.py:19
  416.8 0.0 copy-done.2
  416.8 0.8 multiply_convert_fusion
  (11 shorter events, 0.1 us)
Async XLA Ops:
  6.5 33.5 %all-gather.11.cloned.1.call-start = ((), (), s32[]{:S(2)}) async-start(), calls=%async_computation | async-start | bytes 1310720 | tf_op jit(solution)/shard_map/all_gather | solution.py:36
  9.1 78.2 %all-gather.17.cloned.1.call-start = ((), (), s32[]{:S(2)}) async-start(), calls=%async_computation.3 | async-start | bytes 7864320 | tf_op jit(solution)/shard_map/all_gather | solution.py:30
  9.9 125.4 %all-gather.15.cloned.1.call-start = ((), (), s32[]{:S(2)}) async-start(), calls=%async_computation.2 | async-start | bytes 7864320 | tf_op jit(solution)/shard_map/all_gather | solution.py:29
  10.6 129.5 %copy-start.1 = (f32[3,3,512]{2,1,0:T(4,128)S(1)}, f32[3,3,512]{2,1,0:T(4,128)}, u32[]{:S(2)}) copy-start(f32[3,3,512]{2,1,0:T(4,128)} %param.13) | copy-start | bytes 55300
  10.6 172.5 %all-gather.13.cloned.1.call-start = ((), (), s32[]{:S(2)}) async-start(), calls=%async_computation.1 | async-start | bytes 7864320 | tf_op jit(solution)/shard_map/all_gather | solution.py:28
  11.2 219.7 %all-gather.21.cloned.1.call-start = ((), (), s32[]{:S(2)}) async-start(), calls=%async_computation.5 | async-start | bytes 7864320 | tf_op jit(solution)/shard_map/all_gather | solution.py:31
  11.8 248.6 %all-gather.19.cloned.1.call-start = ((), (), s32[]{:S(2)}) async-start(), calls=%async_computation.4 | async-start | bytes 1310720 | tf_op jit(solution)/shard_map/all_gather | solution.py:57
  40.0 143.1 %copy-start.3 = (bf16[256,2048]{1,0:T(8,128)(2,1)S(1)}, bf16[256,2048]{1,0:T(8,128)(2,1)}, u32[]{:S(2)}) copy-start(bf16[256,2048]{1,0:T(8,128)(2,1)} %all-gather.11.cloned.1.call-done) | copy-start | bytes 3145732
  90.0 170.4 %copy-start = (bf16[256,512]{1,0:T(8,128)(2,1)S(1)}, bf16[256,512]{1,0:T(8,128)(2,1)}, u32[]{:S(2)}) copy-start(bf16[256,512]{1,0:T(8,128)(2,1)} %param.8) | copy-start | bytes 786436
  137.9 45.2 %collective-permute-start = (bf16[2,512]{1,0:T(2,128)(2,1)S(1)}, bf16[2,512]{1,0:T(2,128)(2,1)S(1)}, u32[]{:S(2)}, u32[]{:S(2)}) collective-permute-start(bf16[2,512]{1,0:T(2,128)(2,1)S(1)} %slice.135), channel_id=1, source_target_pairs={{0,4},{4,8},{8,12},{1,5},{5,9},{9,13},{2,6},{6,10},{10,14},{3,7},{... | collective-permute-start | bytes 6152 | tf_op jit(solution)/shard_map/ppermute | solution.py:15
  186.2 105.0 %all-gather.23.cloned.1.call-start = ((), (), s32[]{:S(2)}) async-start(), calls=%async_computation.6 | async-start | bytes 1310720 | tf_op jit(solution)/shard_map/all_gather | solution.py:36
  263.7 68.4 %all-gather.25.cloned.1.call-start = ((), (), s32[]{:S(2)}) async-start(), calls=%async_computation.7 | async-start | bytes 1310720 | tf_op jit(solution)/shard_map/all_gather | solution.py:57
  291.2 7.5 %copy-start.5 = (bf16[256,2048]{1,0:T(8,128)(2,1)S(1)}, bf16[256,2048]{1,0:T(8,128)(2,1)}, u32[]{:S(2)}) copy-start(bf16[256,2048]{1,0:T(8,128)(2,1)} %all-gather.23.cloned.1.call-done) | copy-start | bytes 3145732
  296.6 2.1 collective-permute-start.1
  301.8 61.2 %all-gather.27.cloned.1.call-start = ((), (), s32[]{:S(2)}) async-start(), calls=%async_computation.8 | async-start | bytes 1310720 | tf_op jit(solution)/shard_map/all_gather | solution.py:36
  335.5 68.4 %all-gather.29.cloned.1.call-start = ((), (), s32[]{:S(2)}) async-start(), calls=%async_computation.9 | async-start | bytes 1310720 | tf_op jit(solution)/shard_map/all_gather | solution.py:57
  363.0 7.5 %copy-start.4 = (bf16[256,2048]{1,0:T(8,128)(2,1)S(1)}, bf16[256,2048]{1,0:T(8,128)(2,1)}, u32[]{:S(2)}) copy-start(bf16[256,2048]{1,0:T(8,128)(2,1)} %all-gather.27.cloned.1.call-done) | copy-start | bytes 3145732
  368.4 48.5 %copy-start.2 = (f32[512]{0:T(512)S(1)}, f32[512]{0:T(512)}, u32[]{:S(2)}) copy-start(f32[512]{0:T(512)} %param.15) | copy-start | bytes 6148
  368.4 2.1 collective-permute-start.2
Sparse Core Ops, SparseCore 0:
  9.2 30.7 all-gather.10
  41.6 45.7 all-gather.16
  88.9 46.3 all-gather.14
  136.7 46.3 all-gather.12
  184.5 46.3 all-gather.20
  232.3 27.9 all-gather.18
  263.8 27.3 all-gather.22
  302.0 30.1 all-gather.24
  335.6 27.3 all-gather.26
  373.8 30.1 all-gather.28
where the time goes:
time: 425 us
  waiting for transfers between devices  323 us (76%)
  blocking collectives  44.2 us (10%)
  matrix products  34.6 us (8%)
  between operations  13.7 us (3%)
  starting transfers between devices  5.1 us (1%)
    all_gather x3, waiting for transfers between devices, shards(): spread = lax.all_gather(gated, 'tp', axis=1, tiled=True)  90 us
    all_gather x3, waiting for transfers between devices, shards(): gathered = lax.all_gather(normed, 'tp', axis=1, tiled=True)  49.1 us
    all_gather x1, waiting for transfers between devices, shards(): lax.all_gather(value_proj, 'sp', axis=1, tiled=True)  47.3 us
    all_gather x1, waiting for transfers between devices, shards(): lax.all_gather(in_gate, 'sp', axis=1, tiled=True)  45.3 us
    all_gather x1, waiting for transfers between devices, shards(): lax.all_gather(mix_proj, 'sp', axis=1, tiled=True)  44.6 us
    psum x4, blocking collectives, row_scale(): squares = lax.psum(jnp.sum(stream * stream, axis=1, keepdims=True), 'tp')  44.2 us
    all_gather x1, waiting for transfers between devices, shards(): lax.all_gather(out_gate, 'sp', axis=1, tiled=True)  43 us
    dot_general x9, matrix products, shards(): jnp.dot(gathered, weight[layer_index], preferred_element_type=jnp.float32)  25.2 us
  transfers between devices with their start and end apart: 13, of which 12 were waited for; matrix products, arithmetic and copies ran while one was open for 2% of the time, Pallas kernels for 0%

commit v1 on v0

--- a/solution.py
+++ b/solution.py
@@ -33,7 +33,14 @@
     for layer_index in range(LAYERS):
         scale = row_scale(stream)
         normed = (stream * norm_gains[layer_index]).astype(jnp.bfloat16)
-        gathered = lax.all_gather(normed, "tp", axis=1, tiled=True)
+        ring = [normed]
+        for hop in range(3):
+            ring.append(lax.ppermute(ring[-1], "tp", [(dev, (dev + 1) % 4) for dev in range(4)]))
+        gathered = jnp.roll(
+            jnp.concatenate(ring[::-1], axis=1),
+            (lax.axis_index("tp") + 1) * ring[0].shape[1],
+            axis=1,
+        )
         products = tuple(
             (
                 jnp.dot(gathered, weight[layer_index], preferred_element_type=jnp.float32)

time: 425 us -> 399 us (0.939)
  waiting for transfers between devices: 323 us -> 290 us
  starting transfers between devices: 5.1 us -> 11.1 us
    ppermute x0 -> x9, waiting for transfers between devices: none -> 50.4 us  [shards(): lax.ppermute(ring[-1], 'tp', [(dev, (dev + 1) % 4) for dev in range(4)])]
    all_gather x3 -> x0, waiting for transfers between devices: 49.1 us -> none  [shards(): gathered = lax.all_gather(normed, 'tp', axis=1, tiled=True)]
    all_gather x1, waiting for transfers between devices: 47.3 us -> 14.2 us  [shards(): lax.all_gather(value_proj, 'sp', axis=1, tiled=True)]
    ppermute x0 -> x9, starting transfers between devices: none -> 6.11 us  [shards(): lax.ppermute(ring[-1], 'tp', [(dev, (dev + 1) % 4) for dev in range(4)])]
  transfers between devices with their start and end apart: 13 -> 19, of which waited for: 12 -> 15; matrix products, arithmetic and copies ran while one was open for 2% -> 2% of each run, Pallas kernels for 0% -> 0%
where the time goes in v1:
time: 399 us; the launch traced here: 398 us
  waiting for transfers between devices  290 us (73%)
  blocking collectives  46.6 us (12%)
  matrix products  31.3 us (8%)
  between operations  13.7 us (3%)
  starting transfers between devices  11.1 us (3%)
  other arithmetic  5.01 us (1%)
    all_gather x3, waiting for transfers between devices, shards(): spread = lax.all_gather(gated, 'tp', axis=1, tiled=True)  87.6 us
    ppermute x9, waiting for transfers between devices, shards(): lax.ppermute(ring[-1], 'tp', [(dev, (dev + 1) % 4) for dev in range(4)])  50.4 us
    psum x4, blocking collectives, row_scale(): squares = lax.psum(jnp.sum(stream * stream, axis=1, keepdims=True), 'tp')  46.6 us
    all_gather x1, waiting for transfers between devices, shards(): lax.all_gather(in_gate, 'sp', axis=1, tiled=True)  45.6 us
    all_gather x1, waiting for transfers between devices, shards(): lax.all_gather(mix_proj, 'sp', axis=1, tiled=True)  44.6 us
    all_gather x1, waiting for transfers between devices, shards(): lax.all_gather(out_gate, 'sp', axis=1, tiled=True)  43.4 us
    dot_general x9, matrix products, shards(): jnp.dot(gathered, weight[layer_index], preferred_element_type=jnp.float32)  23.1 us
    all_gather x1, waiting for transfers between devices, shards(): lax.all_gather(value_proj, 'sp', axis=1, tiled=True)  14.2 us
  transfers between devices with their start and end apart: 19, of which 15 were waited for; matrix products, arithmetic and copies ran while one was open for 2% of the time, Pallas kernels for 0%

profile of v1, /device:TPU:0, one launch (start us, length us, event | category | flops | bytes accessed | tf_op | source)
XLA Modules:
  0.0 397.9 jit_solution(16695529249188009231)
XLA Ops:
  6.5 0.7 all-gather.12.cloned.1.call-update
  7.3 0.0 all-gather.10.cloned.1.call-start
  7.3 0.7 all-gather.10.cloned.1.call-update
  8.0 0.0 all-gather.8.cloned.1.call-start
  8.1 0.7 all-gather.8.cloned.1.call-update
  8.8 0.0 all-gather.16.cloned.1.call-start
  8.8 0.5 all-gather.16.cloned.1.call-update
  9.3 0.0 all-gather.14.cloned.1.call-start
  9.4 0.2 fusion.76
  9.6 3.1 collective-permute-start
  12.7 8.3 %collective-permute-done = bf16[256,512]{1,0:T(8,128)(2,1)S(1)} collective-permute-done((bf16[256,512]{1,0:T(8,128)(2,1)S(1)}, bf16[256,512]{1,0:T(8,128)(2,1)S(1)}, u32[]{:S(2)}, u32[]{:S(2)}) %collective-permute-start) | collective-permute-done | bytes 262176 | tf_op jit(solution)/shard_map/ppermute | solution.py:38
  21.0 0.0 collective-permute-start.1
  21.0 9.3 %collective-permute-done.1 = bf16[256,512]{1,0:T(8,128)(2,1)S(1)} collective-permute-done((bf16[256,512]{1,0:T(8,128)(2,1)S(1)}, bf16[256,512]{1,0:T(8,128)(2,1)S(1)}, u32[]{:S(2)}, u32[]{:S(2)}) %collective-permute-start.1) | collective-permute-done | bytes 262176 | tf_op jit(solution)/shard_map/ppermute | solution.py:38
  30.3 0.0 collective-permute-start.2
  30.3 12.2 %psum.28 = f32[256,1]{0,1:T(1,128)S(1)} all-reduce(f32[256,1]{0,1:T(1,128)S(1)} %bitcast.159), channel_id=1, replica_groups=mesh['grp'=2,'sp'=4,'tp'=4] {'tp'}, use_global_device_ids=true, to_apply=%region_1.3 | all-reduce | flops 256 | bytes 2048 | tf_op jit(solution)/shard_map/psum | solution.py:19
  42.4 0.0 collective-permute-done.2
  42.4 1.3 fusion.71
  43.8 14.2 %all-gather.12.cloned.1.call-done = bf16[3,2048,512]{2,1,0:T(8,128)(2,1)} async-done(((bf16[3,512,512]{2,1,0:T(8,128)(2,1)}), bf16[3,2048,512]{2,1,0:T(8,128)(2,1)}) %all-gather.12.cloned.1.call-update) | async-done | bytes 6291472 | tf_op jit(solution)/shard_map/all_gather | solution.py:30
  58.0 2.3 fusion.39
  60.3 0.0 copy-start.1
  60.3 45.6 %all-gather.10.cloned.1.call-done = bf16[3,2048,512]{2,1,0:T(8,128)(2,1)} async-done(((bf16[3,512,512]{2,1,0:T(8,128)(2,1)}), bf16[3,2048,512]{2,1,0:T(8,128)(2,1)}) %all-gather.10.cloned.1.call-update) | async-done | bytes 6291472 | tf_op jit(solution)/shard_map/all_gather | solution.py:29
  106.0 2.3 fusion.38
  108.3 2.2 collective-permute-start.3
  110.5 43.4 %all-gather.8.cloned.1.call-done = bf16[3,2048,512]{2,1,0:T(8,128)(2,1)} async-done(((bf16[3,512,512]{2,1,0:T(8,128)(2,1)}), bf16[3,2048,512]{2,1,0:T(8,128)(2,1)}) %all-gather.8.cloned.1.call-update) | async-done | bytes 6291472 | tf_op jit(solution)/shard_map/all_gather | solution.py:28
  153.9 0.0 collective-permute-done.3
  153.9 3.1 fusion.35
  157.0 0.0 all-gather.14.cloned.1.call-update
  157.0 0.0 all-gather.18.cloned.1.call-start
  157.1 44.6 %all-gather.16.cloned.1.call-done = bf16[3,2048,512]{2,1,0:T(8,128)(2,1)} async-done(((bf16[3,512,512]{2,1,0:T(8,128)(2,1)}), bf16[3,2048,512]{2,1,0:T(8,128)(2,1)}) %all-gather.16.cloned.1.call-update) | async-done | bytes 6291472 | tf_op jit(solution)/shard_map/all_gather | solution.py:31
  201.7 29.4 %all-gather.14.cloned.1.call-done = bf16[256,2048]{1,0:T(8,128)(2,1)} async-done(((bf16[256,512]{1,0:T(8,128)(2,1)}), bf16[256,2048]{1,0:T(8,128)(2,1)}) %all-gather.14.cloned.1.call-update) | async-done | bytes 1048592 | tf_op jit(solution)/shard_map/all_gather | solution.py:64
  231.2 2.7 multiply_reduce_fusion.2
  233.9 1.5 collective-permute-start.4
  235.4 7.9 %collective-permute-done.4 = bf16[256,512]{1,0:T(8,128)(2,1)S(1)} collective-permute-done((bf16[256,512]{1,0:T(8,128)(2,1)S(1)}, bf16[256,512]{1,0:T(8,128)(2,1)S(1)}, u32[]{:S(2)}, u32[]{:S(2)}) %collective-permute-start.4) | collective-permute-done | bytes 262176 | tf_op jit(solution)/shard_map/ppermute | solution.py:38
  243.3 0.0 collective-permute-start.5
  243.3 8.5 %collective-permute-done.5 = bf16[256,512]{1,0:T(8,128)(2,1)S(1)} collective-permute-done((bf16[256,512]{1,0:T(8,128)(2,1)S(1)}, bf16[256,512]{1,0:T(8,128)(2,1)S(1)}, u32[]{:S(2)}, u32[]{:S(2)}) %collective-permute-start.5) | collective-permute-done | bytes 262176 | tf_op jit(solution)/shard_map/ppermute | solution.py:38
  251.8 0.0 collective-permute-start.6
  251.8 12.2 %psum.29 = f32[256,1]{0,1:T(1,128)S(1)} all-reduce(f32[256,1]{0,1:T(1,128)S(1)} %bitcast.182), channel_id=1, replica_groups=mesh['grp'=2,'sp'=4,'tp'=4] {'tp'}, use_global_device_ids=true, to_apply=%region_3.5 | all-reduce | flops 256 | bytes 2048 | tf_op jit(solution)/shard_map/psum | solution.py:19
  264.0 0.0 collective-permute-done.6
  264.0 1.3 fusion.64
  265.3 2.3 fusion.46
  267.6 2.3 fusion.45
  270.0 1.3 collective-permute-start.7
  271.3 0.8 collective-permute-done.7
  272.1 3.1 fusion.42
  275.2 0.0 all-gather.18.cloned.1.call-update
  275.2 0.0 all-gather.20.cloned.1.call-start
  275.3 29.0 %all-gather.18.cloned.1.call-done = bf16[256,2048]{1,0:T(8,128)(2,1)} async-done(((bf16[256,512]{1,0:T(8,128)(2,1)}), bf16[256,2048]{1,0:T(8,128)(2,1)}) %all-gather.18.cloned.1.call-update) | async-done | bytes 1048592 | tf_op jit(solution)/shard_map/all_gather | solution.py:64
  304.3 2.7 multiply_reduce_fusion.1
  307.0 1.5 collective-permute-start.8
  308.5 7.9 %collective-permute-done.8 = bf16[256,512]{1,0:T(8,128)(2,1)S(1)} collective-permute-done((bf16[256,512]{1,0:T(8,128)(2,1)S(1)}, bf16[256,512]{1,0:T(8,128)(2,1)S(1)}, u32[]{:S(2)}, u32[]{:S(2)}) %collective-permute-start.8) | collective-permute-done | bytes 262176 | tf_op jit(solution)/shard_map/ppermute | solution.py:38
  316.5 8.5 %collective-permute-done.9 = bf16[256,512]{1,0:T(8,128)(2,1)S(1)} collective-permute-done((bf16[256,512]{1,0:T(8,128)(2,1)S(1)}, bf16[256,512]{1,0:T(8,128)(2,1)S(1)}, u32[]{:S(2)}, u32[]{:S(2)}) %collective-permute-start.9) | collective-permute-done | bytes 262176 | tf_op jit(solution)/shard_map/ppermute | solution.py:38
  325.0 12.2 %psum.30 = f32[256,1]{0,1:T(1,128)S(1)} all-reduce(f32[256,1]{0,1:T(1,128)S(1)} %bitcast.181), channel_id=1, replica_groups=mesh['grp'=2,'sp'=4,'tp'=4] {'tp'}, use_global_device_ids=true, to_apply=%region_5.7 | all-reduce | flops 256 | bytes 2048 | tf_op jit(solution)/shard_map/psum | solution.py:19
  337.1 0.0 collective-permute-done.10
  337.1 1.3 fusion.57
  338.5 2.3 fusion.53
  340.8 2.3 fusion.52
  343.1 1.3 collective-permute-start.11
  344.4 0.8 collective-permute-done.11
  345.2 3.1 fusion.49
  348.3 0.0 all-gather.20.cloned.1.call-update
  348.3 29.1 %all-gather.20.cloned.1.call-done = bf16[256,2048]{1,0:T(8,128)(2,1)} async-done(((bf16[256,512]{1,0:T(8,128)(2,1)}), bf16[256,2048]{1,0:T(8,128)(2,1)}) %all-gather.20.cloned.1.call-update) | async-done | bytes 1048592 | tf_op jit(solution)/shard_map/all_gather | solution.py:64
  377.4 2.7 multiply_reduce_fusion
  380.1 10.2 %psum.31 = f32[256,1]{0,1:T(1,128)S(1)} all-reduce(f32[256,1]{0,1:T(1,128)S(1)} %bitcast.183), channel_id=1, replica_groups=mesh['grp'=2,'sp'=4,'tp'=4] {'tp'}, use_global_device_ids=true, to_apply=%region_7.9 | all-reduce | flops 256 | bytes 2048 | tf_op jit(solution)/shard_map/psum | solution.py:19
  390.3 0.8 multiply_convert_fusion
  (19 shorter events, 0.1 us)
Async XLA Ops:
  6.5 51.5 %all-gather.12.cloned.1.call-start = ((), (), s32[]{:S(2)}) async-start(), calls=%async_computation.2 | async-start | bytes 7864320 | tf_op jit(solution)/shard_map/all_gather | solution.py:30
  7.3 2.1 copy-start.2
  7.3 2.1 copy-start
  7.3 98.7 %all-gather.10.cloned.1.call-start = ((), (), s32[]{:S(2)}) async-start(), calls=%async_computation.1 | async-start | bytes 7864320 | tf_op jit(solution)/shard_map/all_gather | solution.py:29
  8.0 145.9 %all-gather.8.cloned.1.call-start = ((), (), s32[]{:S(2)}) async-start(), calls=%async_computation | async-start | bytes 7864320 | tf_op jit(solution)/shard_map/all_gather | solution.py:28
  8.8 193.0 %all-gather.16.cloned.1.call-start = ((), (), s32[]{:S(2)}) async-start(), calls=%async_computation.4 | async-start | bytes 7864320 | tf_op jit(solution)/shard_map/all_gather | solution.py:31
  9.3 221.8 %all-gather.14.cloned.1.call-start = ((), (), s32[]{:S(2)}) async-start(), calls=%async_computation.3 | async-start | bytes 1310720 | tf_op jit(solution)/shard_map/all_gather | solution.py:64
  9.6 11.4 %collective-permute-start = (bf16[256,512]{1,0:T(8,128)(2,1)S(1)}, bf16[256,512]{1,0:T(8,128)(2,1)S(1)}, u32[]{:S(2)}, u32[]{:S(2)}) collective-permute-start(bf16[256,512]{1,0:T(8,128)(2,1)S(1)} %get-tuple-element.11), channel_id=1, source_target_pairs={{0,1},{1,2},{2,3},{3,0},{4,5},{5,6},{6,7},{7,4},{8,9},{9,10},{10,1... | collective-permute-start | bytes 786440 | tf_op jit(solution)/shard_map/ppermute | solution.py:38
  21.0 9.3 %collective-permute-start.1 = (bf16[256,512]{1,0:T(8,128)(2,1)S(1)}, bf16[256,512]{1,0:T(8,128)(2,1)S(1)}, u32[]{:S(2)}, u32[]{:S(2)}) collective-permute-start(bf16[256,512]{1,0:T(8,128)(2,1)S(1)} %collective-permute-done), channel_id=1, source_target_pairs={{0,1},{1,2},{2,3},{3,0},{4,5},{5,6},{6,7},{7,4},{8,9},{9,10},{10,1... | collective-permute-start | bytes 786440 | tf_op jit(solution)/shard_map/ppermute | solution.py:38
  30.3 12.2 %collective-permute-start.2 = (bf16[256,512]{1,0:T(8,128)(2,1)S(1)}, bf16[256,512]{1,0:T(8,128)(2,1)S(1)}, u32[]{:S(2)}, u32[]{:S(2)}) collective-permute-start(bf16[256,512]{1,0:T(8,128)(2,1)S(1)} %collective-permute-done.1), channel_id=1, source_target_pairs={{0,1},{1,2},{2,3},{3,0},{4,5},{5,6},{6,7},{7,4},{8,9},{9,10},{10,1... | collective-permute-start | bytes 786440 | tf_op jit(solution)/shard_map/ppermute | solution.py:38
  60.3 50.1 %copy-start.1 = (f32[3,3,512]{2,1,0:T(4,128)S(1)}, f32[3,3,512]{2,1,0:T(4,128)}, u32[]{:S(2)}) copy-start(f32[3,3,512]{2,1,0:T(4,128)} %param.15) | copy-start | bytes 55300
  108.3 45.6 %collective-permute-start.3 = (bf16[2,512]{1,0:T(2,128)(2,1)S(1)}, bf16[2,512]{1,0:T(2,128)(2,1)S(1)}, u32[]{:S(2)}, u32[]{:S(2)}) collective-permute-start(bf16[2,512]{1,0:T(2,128)(2,1)S(1)} %slice.135), channel_id=1, source_target_pairs={{0,4},{4,8},{8,12},{1,5},{5,9},{9,13},{2,6},{6,10},{10,14},{3,7},{... | collective-permute-start | bytes 6152 | tf_op jit(solution)/shard_map/ppermute | solution.py:15
  157.0 147.3 %all-gather.18.cloned.1.call-start = ((), (), s32[]{:S(2)}) async-start(), calls=%async_computation.5 | async-start | bytes 1310720 | tf_op jit(solution)/shard_map/all_gather | solution.py:64
  233.9 9.4 %collective-permute-start.4 = (bf16[256,512]{1,0:T(8,128)(2,1)S(1)}, bf16[256,512]{1,0:T(8,128)(2,1)S(1)}, u32[]{:S(2)}, u32[]{:S(2)}) collective-permute-start(bf16[256,512]{1,0:T(8,128)(2,1)S(1)} %get-tuple-element.9), channel_id=1, source_target_pairs={{0,1},{1,2},{2,3},{3,0},{4,5},{5,6},{6,7},{7,4},{8,9},{9,10},{10,1... | collective-permute-start | bytes 786440 | tf_op jit(solution)/shard_map/ppermute | solution.py:38
  243.3 8.5 %collective-permute-start.5 = (bf16[256,512]{1,0:T(8,128)(2,1)S(1)}, bf16[256,512]{1,0:T(8,128)(2,1)S(1)}, u32[]{:S(2)}, u32[]{:S(2)}) collective-permute-start(bf16[256,512]{1,0:T(8,128)(2,1)S(1)} %collective-permute-done.4), channel_id=1, source_target_pairs={{0,1},{1,2},{2,3},{3,0},{4,5},{5,6},{6,7},{7,4},{8,9},{9,10},{10,1... | collective-permute-start | bytes 786440 | tf_op jit(solution)/shard_map/ppermute | solution.py:38
  251.8 12.2 %collective-permute-start.6 = (bf16[256,512]{1,0:T(8,128)(2,1)S(1)}, bf16[256,512]{1,0:T(8,128)(2,1)S(1)}, u32[]{:S(2)}, u32[]{:S(2)}) collective-permute-start(bf16[256,512]{1,0:T(8,128)(2,1)S(1)} %collective-permute-done.5), channel_id=1, source_target_pairs={{0,1},{1,2},{2,3},{3,0},{4,5},{5,6},{6,7},{7,4},{8,9},{9,10},{10,1... | collective-permute-start | bytes 786440 | tf_op jit(solution)/shard_map/ppermute | solution.py:38
  270.0 2.1 collective-permute-start.7
  275.2 102.2 %all-gather.20.cloned.1.call-start = ((), (), s32[]{:S(2)}) async-start(), calls=%async_computation.6 | async-start | bytes 1310720 | tf_op jit(solution)/shard_map/all_gather | solution.py:64
  307.0 9.4 %collective-permute-start.8 = (bf16[256,512]{1,0:T(8,128)(2,1)S(1)}, bf16[256,512]{1,0:T(8,128)(2,1)S(1)}, u32[]{:S(2)}, u32[]{:S(2)}) collective-permute-start(bf16[256,512]{1,0:T(8,128)(2,1)S(1)} %get-tuple-element.7), channel_id=1, source_target_pairs={{0,1},{1,2},{2,3},{3,0},{4,5},{5,6},{6,7},{7,4},{8,9},{9,10},{10,1... | collective-permute-start | bytes 786440 | tf_op jit(solution)/shard_map/ppermute | solution.py:38
  316.5 8.5 %collective-permute-start.9 = (bf16[256,512]{1,0:T(8,128)(2,1)S(1)}, bf16[256,512]{1,0:T(8,128)(2,1)S(1)}, u32[]{:S(2)}, u32[]{:S(2)}) collective-permute-start(bf16[256,512]{1,0:T(8,128)(2,1)S(1)} %collective-permute-done.8), channel_id=1, source_target_pairs={{0,1},{1,2},{2,3},{3,0},{4,5},{5,6},{6,7},{7,4},{8,9},{9,10},{10,1... | collective-permute-start | bytes 786440 | tf_op jit(solution)/shard_map/ppermute | solution.py:38
  325.0 12.2 %collective-permute-start.10 = (bf16[256,512]{1,0:T(8,128)(2,1)S(1)}, bf16[256,512]{1,0:T(8,128)(2,1)S(1)}, u32[]{:S(2)}, u32[]{:S(2)}) collective-permute-start(bf16[256,512]{1,0:T(8,128)(2,1)S(1)} %collective-permute-done.9), channel_id=1, source_target_pairs={{0,1},{1,2},{2,3},{3,0},{4,5},{5,6},{6,7},{7,4},{8,9},{9,10},{10,1... | collective-permute-start | bytes 786440 | tf_op jit(solution)/shard_map/ppermute | solution.py:38
  343.1 2.1 collective-permute-start.11
  377.4 12.9 %copy-start.3 = (f32[512]{0:T(512)S(1)}, f32[512]{0:T(512)}, u32[]{:S(2)}) copy-start(f32[512]{0:T(512)} %param.17) | copy-start | bytes 6148
Sparse Core Ops, SparseCore 0:
  8.9 49.0 all-gather.11
  59.6 46.3 all-gather.9
  107.5 46.3 all-gather.7
  155.3 46.3 all-gather.15
  203.1 27.9 all-gather.13
  275.3 28.9 all-gather.17
  348.4 28.9 all-gather.19
